TPU v7x, 32 devices: a whole 2x2x4 slice. The times are simulated.
32 devices in a mesh: ep: 8 (over z, y), tp: 4 (over x, core).
Axes of the slice: x: 2, y: 2, z: 4, core: 2. Of those that a mesh axis runs over, the one named last changes fastest.
Arguments:
- value_in: bfloat16 [4096, 1024], P('ep', 'tp'), may hold values from -6 to 6
- gate_in: bfloat16 [4096, 1024], P('ep', 'tp'), may hold values from -6 to 6
- outer_gate: bfloat16 [4096, 1024], P('ep', 'tp'), may hold values from -6 to 6
- conv_weight: bfloat16 [3, 1024], P(None, 'tp'), may hold values from -3.5 to 3.5
- out_weight: bfloat16 [1024, 2048], P('tp'), may hold values from -0.1875 to 0.1875
- moe_tokens: bfloat16 [4096, 2048], P(('ep', 'tp')), may hold values from -6 to 6
- norm_gain: bfloat16 [2048], replicated, may hold values from 0.099609375 to 1.8984375
- routes: int32 [4096, 2], P(('ep', 'tp')), may hold values from 0 to 7, all different within a row; in each aligned block of 128 rows (0 to 127, 128 to 255, ...) at most 48 rows name the same one
- route_weight: float32 [4096, 2], P(('ep', 'tp')), may hold values from 0.1 to 1
- expert_gate: bfloat16 [8, 2048, 6144], P('ep', None, 'tp'), may hold values from -0.125 to 0.125
- expert_up: bfloat16 [8, 2048, 6144], P('ep', None, 'tp'), may hold values from -0.125 to 0.125
- expert_down: bfloat16 [8, 6144, 2048], P('ep', 'tp'), may hold values from -0.078125 to 0.078125
Outputs:
- mixer_out: bfloat16 [4096, 2048], P(('ep', 'tp'))
- moe_out: bfloat16 [4096, 2048], P(('ep', 'tp'))
Inputs may be any that keep to these rules, and one draw needn't show every extreme that they name: `routes`: each row names 2 different experts. Among the rows of one device no expert is named by more than 48 rows, a bound that some blocks reach.
All inputs are finite; a program needn't handle non-finite values.
Results may differ from a plain program's by a relative error of at most 0.012.
Values may be sent and summed in bfloat16 or wider, within the bound.
A program may use at most 128 MiB of HBM per device.

v0:
```python
import functools

import jax
import jax.numpy as jnp
from jax import lax
from jax.experimental import pallas as pl
from jax.experimental.pallas import tpu as pltpu
from jax.sharding import PartitionSpec as P


def extended(x, sides, width):
    for axis, dim in sides:
        size, length = (lax.axis_size(axis), x.shape[dim])
        up = [(i, (i + 1) % size) for i in range(size - 1)]
        down = [(j, i) for i, j in up]
        last = lax.slice_in_dim(x, length - width, length, axis=dim)
        leading = lax.slice_in_dim(x, 0, width, axis=dim)
        before = lax.ppermute(last, axis, up)
        after = lax.ppermute(leading, axis, down)
        x = jnp.concatenate([before, x, after], axis=dim)
    return x


def rounded(values):
    return lax.optimization_barrier(values.astype(jnp.bfloat16)).astype(jnp.float32)


def mixer_half(value_in, gate_in, outer_gate, conv_weight, out_weight):
    product = (value_in.astype(jnp.float32) * gate_in.astype(jnp.float32)).astype(jnp.bfloat16)
    padded = extended(product, (("ep", 0),), 1).astype(jnp.float32)
    taps = conv_weight.astype(jnp.float32)
    convolved = padded[:-2] * taps[0] + padded[1:-1] * taps[1] + padded[2:] * taps[2]
    mixed_rows = (outer_gate.astype(jnp.float32) * convolved).astype(jnp.bfloat16)
    return rounded(jnp.dot(mixed_rows, out_weight, preferred_element_type=jnp.float32)).astype(
        jnp.bfloat16
    )


MESH = pl.DeviceIdType.MESH


def expert_kernel(
    experts, shards, cap, tile,
    sent, gate_hbm, up_hbm, down_hbm, back,
    gate_w, up_w, down_w, slots, hidden, part, core_in, pair, chip_in, total,
    w_sem, own_sem, out_s, out_r, xf_s, xf_r, df_s, df_r, dr_s, dr_r, xr_s, xr_r, bk_s, bk_r,
):
    stages = experts // 2
    high = shards // 2
    me, mine = lax.axis_index("ep"), lax.axis_index("tp")
    low, top = lax.rem(mine, 2), mine // 2
    partner = (me, mine + 1 - 2 * low)
    across = (me, lax.rem(mine + high, shards))
    wide, half = 2 * cap, 2 * high * cap
    own_half = pl.multiple_of(low * half, 16)
    other_half = pl.multiple_of((1 - low) * half, 16)
    own_top = pl.multiple_of(top * wide, 16)
    other_top = pl.multiple_of((1 - top) * wide, 16)

    def to(k):
        return lax.rem(me + k, experts)

    def source(k):
        return lax.rem(me + experts - k, experts)

    def place(k):
        return pl.ds(pl.multiple_of(own_half + own_top + (k % 2) * cap, 16), cap)

    def remote(src, dst, s, r, device):
        return pltpu.make_async_remote_copy(
            src_ref=src, dst_ref=dst, send_sem=s, recv_sem=r, device_id=device, device_id_type=MESH
        )

    loads = [
        pltpu.make_async_copy(a, b, w_sem.at[i])
        for i, (a, b) in enumerate(((gate_hbm, gate_w), (up_hbm, up_w), (down_hbm, down_w)))
    ]
    barrier = pltpu.get_barrier_semaphore()
    for k in range(1, experts):
        pl.semaphore_signal(barrier, inc=1, device_id=(to(k), mine), device_id_type=MESH)
    for device in (partner, across):
        pl.semaphore_signal(barrier, inc=1, device_id=device, device_id_type=MESH)
    for load in loads:
        load.start()
    own_in = pltpu.make_async_copy(sent.at[me], slots.at[0, place(0)], own_sem.at[0])
    own_in.start()
    pl.semaphore_wait(barrier, experts + 1)

    out = [None] + [
        remote(sent.at[to(k)], slots.at[k // 2, place(k)], out_s.at[k], out_r.at[k], (to(k), mine))
        for k in range(1, experts)
    ]
    for copy in out[1:]:
        copy.start()
    x_out = [
        remote(slots.at[k // 2, place(k)], slots.at[k // 2, place(k)], xf_s.at[k], xf_r.at[k], across)
        for k in range(experts)
    ]
    rows = pl.ds(own_half, half)
    d_out = [
        remote(slots.at[j, rows], slots.at[j, rows], df_s.at[j], df_r.at[j], partner)
        for j in range(stages)
    ]
    d_back = [
        remote(part.at[j, pl.ds(other_half, half)], core_in.at[j], dr_s.at[j], dr_r.at[j], partner)
        for j in range(stages)
    ]
    x_back = [
        remote(
            pair.at[k // 2, pl.ds(pl.multiple_of(other_top + (k % 2) * cap, 16), cap)],
            chip_in.at[k // 2, pl.ds((k % 2) * cap, cap)], xr_s.at[k], xr_r.at[k], across,
        )
        for k in range(experts)
    ]
    own_out = pltpu.make_async_copy(total.at[0, pl.ds(0, cap)], back.at[me], own_sem.at[1])
    home = [own_out] + [
        remote(
            total.at[k // 2, pl.ds((k % 2) * cap, cap)], back.at[me], bk_s.at[k], bk_r.at[k],
            (source(k), mine),
        )
        for k in range(1, experts)
    ]

    def arrive(j):
        for k in (2 * j, 2 * j + 1):
            if k == 0:
                own_in.wait()
            else:
                out[k].wait_recv()
            x_out[k].start()

    def spread(j):
        x_out[2 * j].wait_recv()
        x_out[2 * j + 1].wait_recv()
        d_out[j].start()

    def activate(j):
        d_out[j].wait_recv()

        def step(i, carry):
            at = pl.ds(pl.multiple_of(i * tile, tile), tile)
            x = slots[j]
            g = jnp.dot(x, gate_w[:, at], preferred_element_type=jnp.float32)
            u = jnp.dot(x, up_w[:, at], preferred_element_type=jnp.float32)
            hidden[:, at] = (g / (1.0 + jnp.exp(-g)) * u).astype(jnp.bfloat16)
            return carry

        lax.fori_loop(0, gate_w.shape[1] // tile, step, 0)

    def project(j):
        def step(i, carry):
            at = pl.ds(pl.multiple_of(i * tile, tile), tile)
            part[j, :, at] = jnp.dot(
                hidden[...], down_w[:, at], preferred_element_type=jnp.float32
            ).astype(jnp.bfloat16)
            return carry

        lax.fori_loop(0, down_w.shape[1] // tile, step, 0)
        d_back[j].start()

    def add_pair(j, first, count):
        mine_rows = pl.ds(pl.multiple_of(own_half + first, 16), count)
        pair[j, pl.ds(first, count)] = (
            part[j, mine_rows].astype(jnp.float32)
            + core_in[j, pl.ds(first, count)].astype(jnp.float32)
        ).astype(jnp.bfloat16)

    def pair_up(j):
        d_back[j].wait_recv()
        for k in (2 * j, 2 * j + 1):
            add_pair(j, pl.multiple_of(other_top + (k % 2) * cap, 16), cap)
            x_back[k].start()
        add_pair(j, own_top, wide)

    def finish(j):
        for k in (2 * j, 2 * j + 1):
            x_back[k].wait_recv()
            here = pl.ds((k % 2) * cap, cap)
            held = pl.ds(pl.multiple_of(own_top + (k % 2) * cap, 16), cap)
            total[j, here] = (
                pair[j, held].astype(jnp.float32) + chip_in[j, here].astype(jnp.float32)
            ).astype(jnp.bfloat16)
            home[k].start()

    arrive(0)
    spread(0)
    for j in range(stages):
        if j + 1 < stages:
            arrive(j + 1)
        if j == 0:
            loads[0].wait()
            loads[1].wait()
        activate(j)
        if j + 1 < stages:
            spread(j + 1)
        if j >= 1:
            pair_up(j - 1)
        if j >= 2:
            finish(j - 2)
        if j == 0:
            loads[2].wait()
        project(j)
    pair_up(stages - 1)
    if stages >= 2:
        finish(stages - 2)
    finish(stages - 1)
    own_out.wait()
    for k in range(1, experts):
        out[k].wait_send()
        home[k].wait()
    for k in range(experts):
        x_out[k].wait_send()
        x_back[k].wait_send()
    for j in range(stages):
        d_out[j].wait_send()
        d_back[j].wait_send()


def expert_half(
    partial_rows, moe_tokens, norm_gain, routes, route_weight, expert_gate, expert_up, expert_down
):
    row_total, top_count = routes.shape
    features = moe_tokens.shape[1]
    local_units = expert_gate.shape[2]
    experts, shards = lax.axis_size("ep"), lax.axis_size("tp")
    capacity = 3 * top_count * row_total // (2 * experts)
    capacity = -(-capacity // 16) * 16
    slots = experts * capacity
    tokens_f32 = moe_tokens.astype(jnp.float32)
    normed = (
        tokens_f32
        * lax.rsqrt(jnp.mean(tokens_f32 * tokens_f32, axis=-1, keepdims=True) + 1e-06)
        * norm_gain.astype(jnp.float32)
    ).astype(jnp.bfloat16)
    chosen = routes[:, :, None] == jnp.arange(experts, dtype=jnp.int32)[None, None, :]
    named = chosen.any(axis=1).astype(jnp.bfloat16)
    before = jnp.arange(row_total)[:, None] > jnp.arange(row_total)[None, :]
    rank = jnp.dot(before.astype(jnp.bfloat16), named, preferred_element_type=jnp.float32)
    position = jnp.sum(jnp.where(chosen, rank[:, None, :], 0.0), axis=2).astype(jnp.int32)
    slot_ids = routes * capacity + position
    at_slot = slot_ids[:, :, None] == jnp.arange(slots, dtype=jnp.int32)[None, None, :]
    placement = at_slot.any(axis=1).astype(jnp.bfloat16)
    outgoing = jnp.einsum("rs,rd->sd", placement, normed, preferred_element_type=jnp.float32)
    outgoing = outgoing.astype(jnp.bfloat16).reshape(experts, capacity, features)
    outgoing, partial_rows = lax.optimization_barrier((outgoing, partial_rows))
    mixer_out = lax.psum_scatter(partial_rows, "tp", scatter_dimension=0, tiled=True)
    stages, rows = experts // 2, 2 * shards * capacity
    bf16 = jnp.bfloat16
    dma = pltpu.SemaphoreType.DMA
    returned = pl.pallas_call(
        functools.partial(expert_kernel, experts, shards, capacity, 512),
        out_shape=jax.ShapeDtypeStruct((experts, capacity, features), bf16),
        in_specs=[pl.BlockSpec(memory_space=pltpu.VMEM)] + [pl.BlockSpec(memory_space=pl.ANY)] * 3,
        out_specs=pl.BlockSpec(memory_space=pltpu.VMEM),
        scratch_shapes=[
            pltpu.VMEM((features, local_units), bf16),
            pltpu.VMEM((features, local_units), bf16),
            pltpu.VMEM((local_units, features), bf16),
            pltpu.VMEM((stages, rows, features), bf16),
            pltpu.VMEM((rows, local_units), bf16),
            pltpu.VMEM((stages, rows, features), bf16),
            pltpu.VMEM((stages, rows // 2, features), bf16),
            pltpu.VMEM((stages, rows // 2, features), bf16),
            pltpu.VMEM((stages, rows // shards, features), bf16),
            pltpu.VMEM((stages, rows // shards, features), bf16),
            dma((3,)),
            dma((2,)),
        ]
        + [dma((experts,))] * 4
        + [dma((stages,))] * 4
        + [dma((experts,))] * 4,
        compiler_params=pltpu.CompilerParams(
            collective_id=0, has_side_effects=True, vmem_limit_bytes=60 * 2**20
        ),
        cost_estimate=pl.CostEstimate(
            flops=6 * stages * rows * features * local_units,
            bytes_accessed=6 * features * local_units,
            transcendentals=stages * rows * local_units,
        ),
    )(outgoing, expert_gate[0], expert_up[0], expert_down[0])
    weights = jnp.sum(jnp.where(at_slot, route_weight[:, :, None], 0.0), axis=1)
    leading = weights.astype(bf16)
    trailing = (weights - leading.astype(jnp.float32)).astype(bf16)
    result = returned.reshape(slots, features)
    moe_out = jnp.dot(leading, result, preferred_element_type=jnp.float32) + jnp.dot(
        trailing, result, preferred_element_type=jnp.float32
    )
    return mixer_out, moe_out.astype(bf16)


def body(
    value_in,
    gate_in,
    outer_gate,
    conv_weight,
    out_weight,
    moe_tokens,
    norm_gain,
    routes,
    route_weight,
    expert_gate,
    expert_up,
    expert_down,
):
    partial_rows = mixer_half(value_in, gate_in, outer_gate, conv_weight, out_weight)
    return expert_half(
        partial_rows,
        moe_tokens,
        norm_gain,
        routes,
        route_weight,
        expert_gate,
        expert_up,
        expert_down,
    )


def solution(mesh):
    placed = (
        P("ep", "tp"),
        P("ep", "tp"),
        P("ep", "tp"),
        P(None, "tp"),
        P("tp", None),
        P(("ep", "tp"), None),
        P(),
        P(("ep", "tp"), None),
        P(("ep", "tp"), None),
        P("ep", None, "tp"),
        P("ep", None, "tp"),
        P("ep", "tp", None),
    )
    return jax.shard_map(
        body,
        mesh=mesh,
        in_specs=placed,
        out_specs=(P(("ep", "tp"), None), P(("ep", "tp"), None)),
        check_vma=False,
    )
```

profile of v0, /device:TPU:0, one launch (start us, length us, event | category | flops | bytes accessed | tf_op | source)
XLA Modules:
  0.0 148.0 jit_solution(10657339117806072523)
XLA Ops:
  7.2 0.0 copy-start
  7.2 0.0 copy-start.2
  7.2 0.0 reduce-scatter.2.cloned.1.call-start
  7.2 1.2 multiply_convert_fusion
  8.5 0.0 copy-start.4
  8.5 1.3 collective-permute-start.1
  9.8 5.5 %collective-permute-start = (bf16[1,256]{1,0:T(2,128)(2,1)S(1)}, bf16[1,256]{1,0:T(2,128)(2,1)S(1)}, u32[]{:S(2)}, u32[]{:S(2)}) collective-permute-start(bf16[1,256]{1,0:T(2,128)(2,1)S(1)} %get-tuple-element.6), channel_id=1, source_target_pairs={{0,4},{4,8},{8,12},{12,16},{16,20},{20,24},{24,28},{1,5},{5,9},{9,... | collective-permute-start | bytes 1544 | tf_op jit(solution)/shard_map/ppermute | solution.py:18
  15.3 0.7 fusion.20
  16.0 0.1 fusion.16
  16.1 0.7 select_reduce_fusion.1
  16.9 0.7 convert_add_fusion
  17.5 0.1 fusion.11
  17.6 0.7 convert_element_type.58
  18.3 1.2 fusion.1
  19.6 0.0 copy-start.3
  19.6 0.0 copy-done.2
  19.6 1.8 %convolution_convert_fusion.1 = bf16[384,2048]{1,0:T(8,128)(2,1)} fusion(pred[128,384]{1,0:T(8,128)(4,1)S(1)} %fusion.11, bf16[128,2048]{1,0:T(8,128)(2,1)S(1)} %copy-done.2, f32[2048]{0:T(1024)S(1)} %convert_element_type.58, f32[128]{0:T(128)S(1)} %add_rsqrt_fusion), kind=kOutput, calls=%fused_computation.1 | convolution fusion | flops 203161600 | bytes 2155008 | tf_op jit(solution)/shard_map/rs,rd->sd/dot_general | solution.py:243
  21.4 0.0 copy-done.4
  21.4 0.0 collective-permute-done.1
  21.4 0.0 collective-permute-done
  21.4 0.1 maximum_convert_fusion
  21.5 0.0 copy-done
  21.5 0.0 copy-done.3
  21.5 2.2 %convolution_convert_fusion = bf16[512,2048]{1,0:T(8,128)(2,1)} fusion(bf16[256,2048]{1,0:T(8,128)(2,1)S(1)} %copy-done, f32[514,256]{1,0:T(8,128)S(1)} %maximum_convert_fusion, bf16[512,256]{1,0:T(8,128)(2,1)S(1)} %copy-done.3, f32[256]{0:T(256)S(1)} %bitcast.18, f32[256]{0:T(256)S(1)} %bitcast.17, f32[256]{0:T(256)S(1)} %bitcast.16), kind=kOutput, calls=%fused_computation | convolution fusion | flops 538968064 | bytes 4983808 | tf_op jit(solution)/shard_map/dot_general | solution.py:34
  23.7 0.0 copy-start.5
  23.7 0.0 reduce-scatter.2.cloned.1.call-update
  23.7 0.7 copy-done.5
  24.4 0.1 select_reduce_fusion
  24.5 113.4 %shard_map.131 = bf16[8,48,2048]{2,1,0:T(8,128)(2,1)} custom-call(bf16[8,48,2048]{2,1,0:T(8,128)(2,1)} %bitcast.15, bf16[2048,1536]{1,0:T(8,128)(2,1)} %bitcast.19, bf16[2048,1536]{1,0:T(8,128)(2,1)} %bitcast.20, bf16[1536,2048]{1,0:T(8,128)(2,1)} %bitcast.21), custom_call_target="tpu_custom_call" | custom-call | flops 28991029248 | bytes 18874368 | tf_op jit(solution)/shard_map/pallas_call | solution.py:250
  137.9 0.0 copy-start.1
  137.9 2.0 %fusion.18 = f32[128,2048]{1,0:T(8,128)S(1)} fusion(bf16[384,2048]{1,0:T(8,128)(2,1)} %bitcast.13, f32[128,384]{1,0:T(8,128)S(1)} %select_reduce_fusion), kind=kOutput, calls=%fused_computation.30 | convolution fusion | flops 201375744 | bytes 2818048 | tf_op jit(solution)/shard_map/dot_general | solution.py:285
  139.9 0.0 copy-done.1
  139.9 1.2 fusion
  141.1 0.0 reduce-scatter.2.cloned.1.call-done
  (3 shorter events, 0.0 us)
Async XLA Ops:
  7.2 14.3 %copy-start = (bf16[256,2048]{1,0:T(8,128)(2,1)S(1)}, bf16[256,2048]{1,0:T(8,128)(2,1)}, u32[]{:S(2)}) copy-start(bf16[256,2048]{1,0:T(8,128)(2,1)} %param.16) | copy-start | bytes 3145732
  7.2 12.4 %copy-start.2 = (bf16[128,2048]{1,0:T(8,128)(2,1)S(1)}, bf16[128,2048]{1,0:T(8,128)(2,1)}, u32[]{:S(2)}) copy-start(bf16[128,2048]{1,0:T(8,128)(2,1)} %param.17) | copy-start | bytes 1572868
  7.2 134.0 %reduce-scatter.2.cloned.1.call-start = ((), (), s32[]{:S(2)}) async-start(), calls=%async_computation.1 | async-start | bytes 2621440 | tf_op jit(solution)/shard_map/reduce_scatter | solution.py:246
  8.5 13.0 %copy-start.4 = (bf16[3,256]{1,0:T(4,128)(2,1)S(1)}, bf16[3,256]{1,0:T(4,128)(2,1)}, u32[]{:S(2)}) copy-start(bf16[3,256]{1,0:T(4,128)(2,1)} %param.15) | copy-start | bytes 4612
  8.5 12.9 %collective-permute-start.1 = (bf16[1,256]{1,0:T(2,128)(2,1)S(1)}, bf16[1,256]{1,0:T(2,128)(2,1)S(1)}, u32[]{:S(2)}, u32[]{:S(2)}) collective-permute-start(bf16[1,256]{1,0:T(2,128)(2,1)S(1)} %get-tuple-element.7), channel_id=1, source_target_pairs={{4,0},{8,4},{12,8},{16,12},{20,16},{24,20},{28,24},{5,1},{9,5},{13... | collective-permute-start | bytes 1544 | tf_op jit(solution)/shard_map/ppermute | solution.py:19
  9.8 11.6 %collective-permute-start = (bf16[1,256]{1,0:T(2,128)(2,1)S(1)}, bf16[1,256]{1,0:T(2,128)(2,1)S(1)}, u32[]{:S(2)}, u32[]{:S(2)}) collective-permute-start(bf16[1,256]{1,0:T(2,128)(2,1)S(1)} %get-tuple-element.6), channel_id=1, source_target_pairs={{0,4},{4,8},{8,12},{12,16},{16,20},{20,24},{24,28},{1,5},{5,9},{9,... | collective-permute-start | bytes 1544 | tf_op jit(solution)/shard_map/ppermute | solution.py:18
  19.6 1.9 %copy-start.3 = (bf16[512,256]{1,0:T(8,128)(2,1)S(1)}, bf16[512,256]{1,0:T(8,128)(2,1)}, u32[]{:S(2)}) copy-start(bf16[512,256]{1,0:T(8,128)(2,1)} %param.14) | copy-start | bytes 786436
  23.7 0.7 copy-start.5
  137.9 2.0 %copy-start.1 = (bf16[8,48,2048]{2,1,0:T(8,128)(2,1)S(1)}, bf16[8,48,2048]{2,1,0:T(8,128)(2,1)}, u32[]{:S(2)}) copy-start(bf16[8,48,2048]{2,1,0:T(8,128)(2,1)} %shard_map.131) | copy-start | bytes 4718596
Sparse Core Ops, SparseCore 0:
  23.8 38.1 reduce-scatter.1
where the time goes:
time: 149 us; the launch traced here: 148 us
  Pallas kernels  113 us (76%)
  between operations  14.2 us (10%)
  matrix products  7.31 us (5%)
  starting transfers between devices  6.86 us (5%)
  other arithmetic  5.52 us (4%)
    pallas_call x1, Pallas kernels, expert_half(): pl.pallas_call(functools.partial(expert_kernel, experts, shards, capacity...  113 us
    ppermute x1, starting transfers between devices, extended(): before = lax.ppermute(last, axis, up)  5.53 us
  transfers between devices with their start and end apart: 3, of which 0 were waited for; matrix products, arithmetic and copies ran while one was open for 6% of the time, Pallas kernels for 77%

commit v1 on v0

v1 whole, which is shorter than its diff:
```python
import functools

import jax
import jax.numpy as jnp
from jax import lax
from jax.experimental import pallas as pl
from jax.experimental.pallas import tpu as pltpu
from jax.sharding import PartitionSpec as P

MESH = pl.DeviceIdType.MESH
F32, BF16 = jnp.float32, jnp.bfloat16
HALO = 16
PIECES = 4


def moved(at, k, count, back=False):
    if count & (count - 1):
        return lax.rem(at + (count - k if back else k), count)
    bit = 1
    while bit < count:
        if k & bit:
            at = at + bit * (1 - 2 * lax.rem(at // bit, 2))
        bit *= 2
    return at


def paired(experts):
    near, far = list(range(2, experts // 2)), list(range(experts // 2, experts))
    left = far[len(near):]
    return [(0, 1)] + list(zip(far, near)) + list(zip(left[::2], left[1::2]))


def kernel(
    experts, shards, cap, tile,
    value_hbm, gatein_hbm, outer_hbm, conv_ref, outw_hbm, tokens_hbm, gain_ref, routes_ref, rw_ref,
    gate_hbm, up_hbm, down_hbm,
    mixer_ref, moe_ref,
    gate_w, up_w, down_w, value, gatein, outer, outw, tokens,
    normed, sent, weights, slots, hidden, part, core_in, chip_in, back,
    prod, mixed, mpart, mcore, mx_in,
    w_sem, own_sem, out_s, out_r, xf_s, xf_r, df_s, df_r, dr_s, dr_r, xr_s, xr_r, bk_s, bk_r,
    h_s, h_r, md_s, md_r, mx_s, mx_r,
):
    stages = experts // 2
    high = shards // 2
    rows_own, features = tokens.shape
    slot_count = experts * cap
    me, mine = lax.axis_index("ep"), lax.axis_index("tp")
    low, top = lax.rem(mine, 2), mine // 2
    partner = (me, mine + 1 - 2 * low)
    across = (me, lax.rem(mine + high, shards))
    wide, half = 2 * cap, 2 * high * cap
    own_half = pl.multiple_of(low * half, 16)
    other_half = pl.multiple_of((1 - low) * half, 16)
    own_top = pl.multiple_of(top * wide, 16)
    other_top = pl.multiple_of((1 - top) * wide, 16)

    def to(k):
        return moved(me, k, experts)

    def source(k):
        return moved(me, k, experts, True)

    steps = paired(experts)
    stage = {k: j for j, ks in enumerate(steps) for k in ks}
    seat = {k: ks.index(k) * cap for ks in steps for k in ks}

    def place(k):
        return pl.ds(pl.multiple_of(own_half + own_top + seat[k], 16), cap)

    def block(e):
        return pl.ds(pl.multiple_of(e * cap, 16), cap)

    def remote(src, dst, s, r, device):
        return pltpu.make_async_remote_copy(
            src_ref=src, dst_ref=dst, send_sem=s, recv_sem=r, device_id=device, device_id_type=MESH
        )

    loads = [
        pltpu.make_async_copy(a, b, w_sem.at[i])
        for i, (a, b) in enumerate(
            (
                (tokens_hbm, tokens), (value_hbm, value), (gatein_hbm, gatein),
                (outer_hbm, outer), (outw_hbm, outw),
                (gate_hbm, gate_w), (up_hbm, up_w), (down_hbm, down_w),
            )
        )
    ]
    barrier = pltpu.get_barrier_semaphore()
    for k in range(1, experts):
        pl.semaphore_signal(barrier, inc=1, device_id=(to(k), mine), device_id_type=MESH)
    for device in (partner, across):
        pl.semaphore_signal(barrier, inc=1, device_id=device, device_id_type=MESH)
    for load in loads:
        load.start()

    out = [None] + [
        remote(
            sent.at[block(to(k))], slots.at[stage[k], place(k)], out_s.at[k], out_r.at[k],
            (to(k), mine),
        )
        for k in range(1, experts)
    ]
    own_in = pltpu.make_async_copy(sent.at[block(me)], slots.at[0, place(0)], own_sem.at[0])
    x_out = [
        remote(slots.at[stage[k], place(k)], slots.at[stage[k], place(k)], xf_s.at[k], xf_r.at[k], across)
        for k in range(experts)
    ]
    rows = pl.ds(own_half, half)
    d_out = [
        remote(slots.at[j, rows], slots.at[j, rows], df_s.at[j], df_r.at[j], partner)
        for j in range(stages)
    ]
    d_back = [
        remote(part.at[j, pl.ds(other_half, half)], core_in.at[j], dr_s.at[j], dr_r.at[j], partner)
        for j in range(stages)
    ]
    x_back = [
        remote(
            core_in.at[stage[k], pl.ds(pl.multiple_of(other_top + seat[k], 16), cap)],
            chip_in.at[stage[k], pl.ds(seat[k], cap)], xr_s.at[k], xr_r.at[k], across,
        )
        for k in range(experts)
    ]
    own_out = pltpu.make_async_copy(chip_in.at[0, pl.ds(0, cap)], back.at[block(me)], own_sem.at[1])
    home = [own_out] + [
        remote(
            chip_in.at[stage[k], pl.ds(seat[k], cap)], back.at[block(me)],
            bk_s.at[k], bk_r.at[k], (source(k), mine),
        )
        for k in range(1, experts)
    ]
    length = value.shape[0]
    halo = [
        remote(
            prod.at[pl.ds(length, HALO)], prod.at[pl.ds(0, HALO)], h_s.at[0], h_r.at[0],
            (lax.rem(me + 1, experts), mine),
        ),
        remote(
            prod.at[pl.ds(HALO, HALO)], prod.at[pl.ds(length + HALO, HALO)], h_s.at[1], h_r.at[1],
            (lax.rem(me + experts - 1, experts), mine),
        ),
    ]
    owned = length // shards

    def owner_rows(x, core):
        return pl.ds(pl.multiple_of((2 * x + core) * owned, 16), owned)

    m_core = [
        remote(
            mpart.at[owner_rows(x, 1 - low)], mcore.at[x], md_s.at[x], md_r.at[x], partner
        )
        for x in range(high)
    ]
    piece = owned // PIECES
    m_across = [
        remote(
            mcore.at[1 - top, pl.ds(i * piece, piece)], mx_in.at[pl.ds(i * piece, piece)],
            mx_s.at[i], mx_r.at[i], across,
        )
        for i in range(PIECES)
    ]

    loads[0].wait()
    gain = gain_ref[...].astype(F32)

    def norm(i, carry):
        at = pl.ds(pl.multiple_of(i * 16, 16), 16)
        x = tokens[at, :].astype(F32)
        scale = lax.rsqrt(jnp.mean(x * x, axis=-1, keepdims=True) + 1e-06)
        normed[at, :] = (x * scale * gain).astype(BF16)
        return carry

    lax.fori_loop(0, rows_own // 16, norm, 0)
    width = 128 * (-(-experts // 128))
    lanes = lax.broadcasted_iota(jnp.int32, (rows_own, width), 1)
    first, second = routes_ref[:, 0:1], routes_ref[:, 1:2]
    is_first = (lanes == first).astype(F32)
    is_second = (lanes == second).astype(F32)
    named = (is_first + is_second).astype(BF16)
    before = (
        lax.broadcasted_iota(jnp.int32, (rows_own, rows_own), 0)
        > lax.broadcasted_iota(jnp.int32, (rows_own, rows_own), 1)
    )
    rank = jnp.dot(before.astype(F32).astype(BF16), named, preferred_element_type=F32)
    slot_lanes = lax.broadcasted_iota(jnp.int32, (rows_own, slot_count), 1).astype(F32)

    def at_slot(route, chosen):
        position = jnp.sum(chosen * rank, axis=1, keepdims=True)
        return (slot_lanes == route.astype(F32) * cap + position).astype(F32)

    at_first, at_second = at_slot(first, is_first), at_slot(second, is_second)
    placement = (at_first + at_second).astype(BF16)

    def gather(i, carry):
        at = pl.ds(pl.multiple_of(i * tile, tile), tile)
        sent[:, at] = lax.dot_general(
            placement, normed[:, at], (((0,), (0,)), ((), ())), preferred_element_type=F32
        ).astype(BF16)
        return carry

    lax.fori_loop(0, features // tile, gather, 0)
    mix = at_first * rw_ref[:, 0:1] + at_second * rw_ref[:, 1:2]
    leading = mix.astype(BF16)
    weights[pl.ds(0, rows_own), :] = leading
    weights[pl.ds(rows_own, rows_own), :] = (mix - leading.astype(F32)).astype(BF16)

    loads[1].wait()
    loads[2].wait()
    prod[pl.ds(HALO, length), :] = (value[...].astype(F32) * gatein[...].astype(F32)).astype(BF16)
    pl.semaphore_wait(barrier, experts + 1)
    for copy in halo:
        copy.start()
    own_in.start()
    for ks in steps[1:] + [(1,)]:
        for k in ks:
            out[k].start()
    own_in.wait()
    x_out[0].start()

    loads[3].wait()
    loads[4].wait()
    for copy in halo:
        copy.wait()
    keep_first = jnp.where(me == 0, 0.0, 1.0)
    keep_last = jnp.where(me == experts - 1, 0.0, 1.0)
    prod[pl.ds(0, HALO), :] = (prod[pl.ds(0, HALO), :].astype(F32) * keep_first).astype(BF16)
    last = pl.ds(length + HALO, HALO)
    prod[last, :] = (prod[last, :].astype(F32) * keep_last).astype(BF16)
    taps = conv_ref[...].astype(F32)

    def mix_rows(x, core):
        start = pl.multiple_of((2 * x + core) * owned, 16)
        span = owned + 2 * HALO
        p = prod[pl.ds(start, span), :].astype(F32)
        convolved = (
            pltpu.roll(p, 1, 0) * taps[0:1] + p * taps[1:2] + pltpu.roll(p, span - 1, 0) * taps[2:3]
        )[HALO:HALO + owned]
        mixed[...] = (outer[pl.ds(start, owned), :].astype(F32) * convolved).astype(BF16)

        def step(i, carry):
            at = pl.ds(pl.multiple_of(i * tile, tile), tile)
            mpart[pl.ds(start, owned), at] = jnp.dot(
                mixed[...], outw[:, at], preferred_element_type=F32
            ).astype(BF16)
            return carry

        lax.fori_loop(0, features // tile, step, 0)

    for x in range(high):
        mix_rows(x, 1 - low)
        m_core[x].start()

    def arrive(k):
        out[k].wait_recv()
        x_out[k].start()

    arrive(1)
    for x in range(high):
        mix_rows(x, low)
    for x in range(high):
        m_core[x].wait_recv()

    def sum_across(i):
        at = pl.ds(i * piece, piece)
        theirs = pl.ds(pl.multiple_of((2 * (1 - top) + low) * owned + i * piece, 16), piece)
        mcore[1 - top, at] = (
            mcore[1 - top, at].astype(F32) + mpart[theirs, :].astype(F32)
        ).astype(BF16)

    for i in range(PIECES):
        sum_across(i)
    m_across[0].start()

    def spread(j):
        for k in steps[j]:
            x_out[k].wait_recv()
        d_out[j].start()

    def activate(j, hooks):
        d_out[j].wait_recv()

        def step(i, carry):
            for at_step, hook in hooks:
                @pl.when(i == at_step)
                def _():
                    hook()

            at = pl.ds(pl.multiple_of(i * tile, tile), tile)
            x = slots[j]
            g = jnp.dot(x, gate_w[:, at], preferred_element_type=F32)
            u = jnp.dot(x, up_w[:, at], preferred_element_type=F32)
            hidden[:, at] = (g / (1.0 + jnp.exp(-g)) * u).astype(BF16)
            return carry

        lax.fori_loop(0, gate_w.shape[1] // tile, step, 0)

    def project(j):
        def step(i, carry):
            at = pl.ds(pl.multiple_of(i * tile, tile), tile)
            part[j, :, at] = jnp.dot(
                hidden[...], down_w[:, at], preferred_element_type=F32
            ).astype(BF16)
            return carry

        lax.fori_loop(0, down_w.shape[1] // tile, step, 0)
        d_back[j].start()

    def pair_up(j):
        d_back[j].wait_recv()
        for k in steps[j]:
            def step(i, carry):
                first = pl.multiple_of(other_top + seat[k] + i * 16, 16)
                at = pl.ds(first, 16)
                theirs = pl.ds(pl.multiple_of(own_half + first, 16), 16)
                core_in[j, at] = (
                    part[j, theirs].astype(F32) + core_in[j, at].astype(F32)
                ).astype(BF16)
                return carry

            lax.fori_loop(0, cap // 16, step, 0)
            x_back[k].start()

    def finish(k):
        j = stage[k]
        x_back[k].wait_recv()

        def step(i, carry):
            here = pl.ds(pl.multiple_of(seat[k] + i * 16, 16), 16)
            first = pl.multiple_of(own_top + seat[k] + i * 16, 16)
            held = pl.ds(pl.multiple_of(own_half + first, 16), 16)
            chip_in[j, here] = (
                part[j, held].astype(F32)
                + core_in[j, pl.ds(first, 16)].astype(F32)
                + chip_in[j, here].astype(F32)
            ).astype(BF16)
            return carry

        lax.fori_loop(0, cap // 16, step, 0)
        home[k].start()

    def arrive_all(j):
        for k in steps[j] if j < stages else ():
            arrive(k)

    arrive_all(1)
    spread(0)
    for i in range(stages):
        hooks = []
        if i == stages - 2:
            hooks.append((1, functools.partial(arrive, steps[-1][1])))
        if i >= 2:
            hooks.append((2, functools.partial(pair_up, i - 1)))
        if i == 0:
            loads[5].wait()
            loads[6].wait()
        activate(i, hooks)
        if i + 2 == stages - 1:
            arrive(steps[-1][0])
        else:
            arrive_all(i + 2)
        if i >= 3:
            for k in steps[i - 2]:
                finish(k)
        if i >= 1 and i + 1 < stages:
            spread(i + 1)
        if i == 0:
            loads[7].wait()
        project(i)
        if i == 0:
            spread(1)
    pair_up(stages - 1)
    pair_up(0)
    for i in range(1, PIECES):
        m_across[i].start()
    for j in (stages - 2, stages - 1, 0):
        for k in steps[j]:
            finish(k)

    for i in range(PIECES):
        m_across[i].wait_recv()
    mine_rows = pl.multiple_of(mine * owned, 16)

    def sum_own(i, carry):
        at = pl.ds(pl.multiple_of(i * 16, 16), 16)
        mixer_ref[at, :] = (
            mpart[pl.ds(pl.multiple_of(mine_rows + i * 16, 16), 16), :].astype(F32)
            + mcore[top, at].astype(F32)
            + mx_in[at, :].astype(F32)
        ).astype(BF16)
        return carry

    lax.fori_loop(0, owned // 16, sum_own, 0)
    own_out.wait()
    for k in range(1, experts):
        home[k].wait()

    def combine(i, carry):
        at = pl.ds(pl.multiple_of(i * tile, tile), tile)
        both = jnp.dot(weights[...], back[:, at], preferred_element_type=F32)
        moe_ref[:, at] = (both[:rows_own] + both[rows_own:]).astype(BF16)
        return carry

    lax.fori_loop(0, features // tile, combine, 0)
    for k in range(1, experts):
        out[k].wait_send()
    for k in range(experts):
        x_out[k].wait_send()
        x_back[k].wait_send()
    for j in range(stages):
        d_out[j].wait_send()
        d_back[j].wait_send()
    for copy in m_core + m_across:
        copy.wait_send()


def body(
    value_in, gate_in, outer_gate, conv_weight, out_weight, moe_tokens, norm_gain, routes,
    route_weight, expert_gate, expert_up, expert_down,
):
    row_total, top_count = routes.shape
    features = moe_tokens.shape[1]
    length, channels = value_in.shape
    local_units = expert_gate.shape[2]
    experts, shards = lax.axis_size("ep"), lax.axis_size("tp")
    capacity = 3 * top_count * row_total // (2 * experts)
    capacity = -(-capacity // 16) * 16
    slots = experts * capacity
    stages, rows = experts // 2, 2 * shards * capacity
    owned = length // shards
    dma = pltpu.SemaphoreType.DMA
    vmem, hbm = pl.BlockSpec(memory_space=pltpu.VMEM), pl.BlockSpec(memory_space=pl.ANY)
    return pl.pallas_call(
        functools.partial(kernel, experts, shards, capacity, 512),
        out_shape=(
            jax.ShapeDtypeStruct((owned, features), BF16),
            jax.ShapeDtypeStruct((row_total, features), BF16),
        ),
        in_specs=[hbm, hbm, hbm, vmem, hbm, hbm, vmem, vmem, vmem, hbm, hbm, hbm],
        out_specs=(vmem, vmem),
        scratch_shapes=[
            pltpu.VMEM((features, local_units), BF16),
            pltpu.VMEM((features, local_units), BF16),
            pltpu.VMEM((local_units, features), BF16),
            pltpu.VMEM((length, channels), BF16),
            pltpu.VMEM((length, channels), BF16),
            pltpu.VMEM((length, channels), BF16),
            pltpu.VMEM((channels, features), BF16),
            pltpu.VMEM((row_total, features), BF16),
            pltpu.VMEM((row_total, features), BF16),
            pltpu.VMEM((slots, features), BF16),
            pltpu.VMEM((2 * row_total, slots), BF16),
            pltpu.VMEM((stages, rows, features), BF16),
            pltpu.VMEM((rows, local_units), BF16),
            pltpu.VMEM((stages, rows, features), BF16),
            pltpu.VMEM((stages, rows // 2, features), BF16),
            pltpu.VMEM((stages, rows // shards, features), BF16),
            pltpu.VMEM((slots, features), BF16),
            pltpu.VMEM((length + 2 * HALO, channels), BF16),
            pltpu.VMEM((owned, channels), BF16),
            pltpu.VMEM((length, features), BF16),
            pltpu.VMEM((shards // 2, owned, features), BF16),
            pltpu.VMEM((owned, features), BF16),
            dma((8,)),
            dma((2,)),
        ]
        + [dma((experts,))] * 4
        + [dma((stages,))] * 4
        + [dma((experts,))] * 4
        + [dma((2,))] * 4
        + [dma((PIECES,))] * 2,
        compiler_params=pltpu.CompilerParams(
            collective_id=0, has_side_effects=True, vmem_limit_bytes=67043328
        ),
        cost_estimate=pl.CostEstimate(
            flops=6 * stages * rows * features * local_units,
            bytes_accessed=6 * features * local_units,
            transcendentals=stages * rows * local_units,
        ),
    )(
        value_in, gate_in, outer_gate, conv_weight, out_weight, moe_tokens,
        norm_gain.reshape(1, features), routes, route_weight,
        expert_gate[0], expert_up[0], expert_down[0],
    )


def solution(mesh):
    placed = (
        P("ep", "tp"),
        P("ep", "tp"),
        P("ep", "tp"),
        P(None, "tp"),
        P("tp", None),
        P(("ep", "tp"), None),
        P(),
        P(("ep", "tp"), None),
        P(("ep", "tp"), None),
        P("ep", None, "tp"),
        P("ep", None, "tp"),
        P("ep", "tp", None),
    )
    return jax.shard_map(
        body,
        mesh=mesh,
        in_specs=placed,
        out_specs=(P(("ep", "tp"), None), P(("ep", "tp"), None)),
        check_vma=False,
    )
```

time: 149 us -> 106 us (0.71)
  Pallas kernels: 113 us -> 97.5 us
  between operations: 14.2 us -> 0.64 us
  matrix products: 7.31 us -> 0 us
  local copies, waits for them, and re-layouts: 0.7 us -> 7.88 us
  starting transfers between devices: 6.86 us -> 0 us
  other arithmetic: 5.52 us -> 0 us
    pallas_call x1, Pallas kernels: 113 us -> 97.5 us  [body(): pl.pallas_call(functools.partial(kernel, experts, shards, capacity, 512),...]
    dot_general x5 -> x0, matrix products: 7.31 us -> none  [the longest x1 2.17 us: mixer_half(): jnp.dot(mixed_rows, out_weight, preferred_element_type=jnp.float32)]
    ppermute x2 -> x0, starting transfers between devices: 6.82 us -> none  [the longest x1 5.53 us: extended(): before = lax.ppermute(last, axis, up)]
    unnamed x12 -> x4, local copies, waits for them, and re-layouts: 0.68 us -> 6.59 us
    reduce_sum x3 -> x0, other arithmetic: 2.08 us -> none  [the longest x1 1.23 us: expert_half(): jnp.mean(tokens_f32 * tokens_f32, axis=-1, keepdims=True) + 1e-06]
    convert_element_type x3 -> x0, other arithmetic: 1.97 us -> none  [the longest x1 1.21 us: mixer_half(): (value_in.astype(jnp.float32) * gate_in.astype(jnp.float32)).astype(jnp.b...]
  transfers between devices with their start and end apart: 3 -> 0, of which waited for: 0 -> 0; matrix products, arithmetic and copies ran while one was open for 6% -> 0% of each run, Pallas kernels for 77% -> 0%
where the time goes in v1:
time: 106 us
  Pallas kernels  97.5 us (92%)
  local copies, waits for them, and re-layouts  7.88 us (7%)
    pallas_call x1, Pallas kernels, body(): pl.pallas_call(functools.partial(kernel, experts, shards, capacity, 512),...  97.5 us
    unnamed x4, local copies, waits for them, and re-layouts  6.59 us

profile of v1, /device:TPU:0, one launch (start us, length us, event | category | flops | bytes accessed | tf_op | source)
XLA Modules:
  0.0 106.0 jit_solution(13163914123109236804)
XLA Ops:
  0.6 1.3 %reshape.7.gain_ref = bf16[1,2048]{1,0:T(2,128)(2,1)} reshape(bf16[2048]{0:T(1024)(128)(2,1)} %param.18) | data formatting | bytes 8192 | tf_op jit(solution)/shard_map/reshape | solution.py:482
  1.9 1.4 %copy.14.routes_ref = s32[128,2]{1,0:T(8,128)} copy(s32[128,2]{0,1:T(2,128)} %param.19) | data formatting | bytes 2048 | tf_op args[7]
  3.3 1.4 %copy.15.rw_ref = f32[128,2]{1,0:T(8,128)} copy(f32[128,2]{0,1:T(2,128)} %param.20) | data formatting | bytes 2048 | tf_op args[8]
  4.7 97.5 %shard_map.131 = (bf16[128,2048]{1,0:T(8,128)(2,1)}, bf16[128,2048]{1,0:T(8,128)(2,1)}) custom-call(bf16[512,256]{1,0:T(8,128)(2,1)} %value_hbm.1, bf16[512,256]{1,0:T(8,128)(2,1)} %gatein_hbm.1, bf16[512,256]{1,0:T(8,128)(2,1)} %outer_hbm.1, bf16[3,256]{1,0:T(4,128)(2,1)} %conv_ref.1, bf16[256,2048]{1,0:T(8,128)(2,1)} %outw_hbm.1, ...), custom_call_target="tpu_custom_call" | custom-call | flops 28991029248 | bytes 18874368 | tf_op jit(solution)/shard_map/pallas_call | solution.py:433
  102.3 1.9 %copy.18 = bf16[128,2048]{1,0:T(8,128)(2,1)} copy(bf16[128,2048]{1,0:T(8,128)(2,1)} %get-tuple-element.4) | data formatting | bytes 1048576
  104.1 1.9 %copy.19 = bf16[128,2048]{1,0:T(8,128)(2,1)} copy(bf16[128,2048]{1,0:T(8,128)(2,1)} %get-tuple-element.5) | data formatting | bytes 1048576

commit v2 on v1

v2 whole, which is shorter than its diff:
```python
import functools

import jax
import jax.numpy as jnp
from jax import lax
from jax.experimental import pallas as pl
from jax.experimental.pallas import tpu as pltpu
from jax.sharding import PartitionSpec as P

MESH = pl.DeviceIdType.MESH
F32, BF16 = jnp.float32, jnp.bfloat16
HALO = 16
PIECES = (1, 3)


def moved(at, k, count, back=False):
    if count & (count - 1):
        return lax.rem(at + (count - k if back else k), count)
    bit = 1
    while bit < count:
        if k & bit:
            at = at + bit * (1 - 2 * lax.rem(at // bit, 2))
        bit *= 2
    return at


def paired(experts):
    near, far = list(range(2, experts // 2)), list(range(experts // 2, experts))
    steps = [(0, 1)]
    for i in range(0, len(near), 2):
        steps += [(far[i],), (far[i + 1],), tuple(near[i:i + 2])]
    return steps + [(k,) for k in far[len(near):]]


def sequence(experts):
    near, far = list(range(2, experts // 2)), list(range(experts // 2, experts))
    both = [k for pair in zip(far, near) for k in pair]
    return both + far[len(near):]


def kernel(
    experts, shards, cap, tile,
    value_hbm, gatein_hbm, outer_hbm, conv_hbm, outw_hbm, tokens_hbm, gain_hbm, routes_hbm, rw_hbm,
    gate_hbm, up_hbm, down_hbm,
    mixer_ref, moe_ref,
    gate_w, up_w, down_w, value, gatein, outer, outw, tokens, conv_ref, gain_ref, routes_ref, rw_ref,
    routes_in, rw_in, normed, sent, weights, weights_in, slots, hidden, part, core_in, chip_in,
    back, back_in, cross_out, cross_in,
    prod, mixed, mpart, mcore, mx_in,
    w_sem, own_sem, out_s, out_r, xf_s, xf_r, df_s, df_r, dr_s, dr_r, xr_s, xr_r, bk_s, bk_r,
    h_s, h_r, md_s, md_r, mx_s, mx_r, rt_s, rt_r, pk_s, pk_r, cx_s, cx_r,
):
    high = shards // 2
    rows_own, features = tokens.shape
    slot_count = experts * cap
    me, mine = lax.axis_index("ep"), lax.axis_index("tp")
    low, top = lax.rem(mine, 2), mine // 2
    partner = (me, mine + 1 - 2 * low)
    across = (me, lax.rem(mine + high, shards))

    def to(k):
        return moved(me, k, experts)

    def source(k):
        return moved(me, k, experts, True)

    steps = paired(experts)
    stages = len(steps)
    stage = {k: j for j, ks in enumerate(steps) for k in ks}
    seat = {k: ks.index(k) * cap for ks in steps for k in ks}
    wide = [cap * len(ks) for ks in steps]
    half = [high * w for w in wide]
    base = [2 * sum(half[:j]) for j in range(stages)]
    part_base = [sum(half[:j]) for j in range(stages)]

    near = experts // 2
    first_near = (me // near) * near

    def rows_at(first, count):
        return pl.ds(pl.multiple_of(first, 16), count)

    def own_rows(j):
        return base[j] + low * half[j]

    def place(k):
        j = stage[k]
        return rows_at(own_rows(j) + top * wide[j] + seat[k], cap)

    def block(e):
        return pl.ds(pl.multiple_of(e * cap, 16), cap)

    def remote(src, dst, s, r, device):
        return pltpu.make_async_remote_copy(
            src_ref=src, dst_ref=dst, send_sem=s, recv_sem=r, device_id=device, device_id_type=MESH
        )

    barrier = pltpu.get_barrier_semaphore()
    for k in range(1, experts):
        pl.semaphore_signal(barrier, inc=1, device_id=(to(k), mine), device_id_type=MESH)
    for device in (partner, across):
        pl.semaphore_signal(barrier, inc=1, device_id=device, device_id_type=MESH)
    wanted = (
        (tokens_hbm, tokens), (gain_hbm, gain_ref), (routes_hbm, routes_ref),
        (value_hbm, value), (gatein_hbm, gatein), (outer_hbm, outer), (outw_hbm, outw),
        (conv_hbm, conv_ref), (rw_hbm, rw_ref),
        (gate_hbm, gate_w), (up_hbm, up_w), (down_hbm, down_w),
    )
    loads = [pltpu.make_async_copy(a, b, w_sem.at[i]) for i, (a, b) in enumerate(wanted)]
    for load in loads:
        load.start()

    out = [None] + [
        remote(
            sent.at[block(to(k))], slots.at[place(k)], out_s.at[k], out_r.at[k],
            (to(k), mine),
        )
        for k in range(1, experts)
    ]
    own_in = pltpu.make_async_copy(sent.at[block(me)], slots.at[place(0)], own_sem.at[0])
    groups = [(k,) for k in range(experts)]

    def crossing(i, ks):
        j = stage[ks[0]]
        here = slots.at[rows_at(own_rows(j) + top * wide[j] + seat[ks[0]], cap * len(ks))]
        return remote(
            here if ks[0] else sent.at[block(me)], here, xf_s.at[i], xf_r.at[i], across
        )

    x_out = {ks: crossing(i, ks) for i, ks in enumerate(groups)}

    def to_partner(j):
        here = slots.at[rows_at(own_rows(j), half[j])]
        return remote(here, here, df_s.at[j], df_r.at[j], partner)

    d_out = [to_partner(j) for j in range(stages)]
    d_back = [
        remote(
            part.at[rows_at(base[j] + (1 - low) * half[j], half[j])],
            core_in.at[rows_at(part_base[j], half[j])], dr_s.at[j], dr_r.at[j], partner,
        )
        for j in range(stages)
    ]
    def core_rows(k, of):
        j = stage[k]
        return core_in.at[rows_at(part_base[j] + of * wide[j] + seat[k], cap)]

    def chip_rows(k):
        return rows_at((k - near) * cap, cap)

    x_back = {
        k: remote(
            core_rows(k, 1 - top), chip_in.at[chip_rows(k)],
            xr_s.at[k - near], xr_r.at[k - near], across,
        )
        for k in range(near, experts)
    }
    home = {
        k: remote(
            chip_in.at[chip_rows(k)] if k >= near else core_rows(k, top), back.at[block(me)],
            bk_s.at[k], bk_r.at[k], (source(k), mine),
        )
        for k in range(1, experts)
    }
    home_in = {
        k: remote(
            core_rows(k, 1 - top), back_in.at[block(me - first_near)],
            pk_s.at[k], pk_r.at[k], (source(k), mine),
        )
        for k in range(1, near)
    }
    cross = remote(cross_out, cross_in, cx_s.at[0], cx_r.at[0], across)
    routing = [
        remote(routes_ref, routes_in, rt_s.at[0], rt_r.at[0], across),
        remote(rw_ref, rw_in, rt_s.at[1], rt_r.at[1], across),
    ]
    length = value.shape[0]
    halo = [
        remote(
            prod.at[pl.ds(length, HALO)], prod.at[pl.ds(0, HALO)], h_s.at[0], h_r.at[0],
            (lax.rem(me + 1, experts), mine),
        ),
        remote(
            prod.at[pl.ds(HALO, HALO)], prod.at[pl.ds(length + HALO, HALO)], h_s.at[1], h_r.at[1],
            (lax.rem(me + experts - 1, experts), mine),
        ),
    ]
    owned = length // shards

    def owner_rows(x, core):
        return pl.ds(pl.multiple_of((2 * x + core) * owned, 16), owned)

    m_core = [
        remote(
            mpart.at[owner_rows(x, 1 - low)], mcore.at[x], md_s.at[x], md_r.at[x], partner
        )
        for x in range(high)
    ]
    unit = owned // sum(PIECES)
    pieces = [pl.ds(sum(PIECES[:i]) * unit, count * unit) for i, count in enumerate(PIECES)]
    m_across = [
        remote(mcore.at[1 - top, at], mx_in.at[at], mx_s.at[i], mx_r.at[i], across)
        for i, at in enumerate(pieces)
    ]

    for load in loads[:3]:
        load.wait()
    gain = gain_ref[...].astype(F32).reshape(1, features)

    def norm(i, carry):
        at = pl.ds(pl.multiple_of(i * 32, 32), 32)
        x = tokens[at, :].astype(F32)
        scale = lax.rsqrt(jnp.mean(x * x, axis=-1, keepdims=True) + 1e-06)
        normed[at, :] = (x * scale * gain).astype(BF16)
        return carry

    lax.fori_loop(0, rows_own // 32, norm, 0)
    lines = 16 * (-(-experts // 16))
    expert_ids = lax.broadcasted_iota(jnp.int32, (lines, rows_own), 0)
    before = (
        lax.broadcasted_iota(jnp.int32, (rows_own, rows_own), 0)
        < lax.broadcasted_iota(jnp.int32, (rows_own, rows_own), 1)
    ).astype(F32).astype(BF16)

    def slots_of(routes, start, count):
        chosen = [(expert_ids == routes[i:i + 1, :]).astype(F32) for i in range(2)]
        named = (chosen[0] + chosen[1]).astype(BF16)
        rank = jnp.dot(named, before, preferred_element_type=F32)
        ids = (lax.broadcasted_iota(jnp.int32, (count, rows_own), 0) + start).astype(F32)

        def at_slot(i):
            position = jnp.sum(chosen[i] * rank, axis=0, keepdims=True)
            return (ids == routes[i:i + 1, :].astype(F32) * cap + position).astype(F32)

        return at_slot(0), at_slot(1)

    def weigh(ref, at_first, at_second, rw):
        mix = at_first * rw[0:1, :] + at_second * rw[1:2, :]
        leading = mix.astype(BF16).astype(F32)
        ref[pl.ds(0, rows_own), :] = leading.T.astype(BF16)
        ref[pl.ds(rows_own, rows_own), :] = (mix - leading).T.astype(BF16)

    at_first, at_second = slots_of(routes_ref[...], 0, slot_count)
    placement = (at_first + at_second).astype(BF16)

    def gather(i, carry):
        at = pl.ds(pl.multiple_of(i * tile, tile), tile)
        sent[:, at] = jnp.dot(
            placement, normed[:, at], preferred_element_type=F32
        ).astype(BF16)
        return carry

    lax.fori_loop(0, features // tile, gather, 0)
    loads[3].wait()
    loads[4].wait()

    def multiply(first, count):
        at = pl.ds(first, count)
        prod[pl.ds(HALO + first, count), :] = (
            value[at, :].astype(F32) * gatein[at, :].astype(F32)
        ).astype(BF16)

    multiply(0, HALO)
    multiply(length - HALO, HALO)
    pl.semaphore_wait(barrier, experts + 1)
    x_out[0,].start()
    loads[8].wait()
    for copy in routing:
        copy.start()
    for copy in halo:
        copy.start()
    for k in sequence(experts) + [1]:
        out[k].start()
    own_in.start()

    multiply(HALO, length - 2 * HALO)
    for load in loads[5:8]:
        load.wait()
    for copy in halo:
        copy.wait()
    keep_first = jnp.where(me == 0, 0.0, 1.0)
    keep_last = jnp.where(me == experts - 1, 0.0, 1.0)
    prod[pl.ds(0, HALO), :] = (prod[pl.ds(0, HALO), :].astype(F32) * keep_first).astype(BF16)
    last = pl.ds(length + HALO, HALO)
    prod[last, :] = (prod[last, :].astype(F32) * keep_last).astype(BF16)
    taps = conv_ref[...].astype(F32)

    def mix_rows(x, core):
        start = pl.multiple_of((2 * x + core) * owned, 16)
        span = owned + 2 * HALO
        p = prod[pl.ds(start, span), :].astype(F32)
        convolved = (
            pltpu.roll(p, 1, 0) * taps[0:1] + p * taps[1:2] + pltpu.roll(p, span - 1, 0) * taps[2:3]
        )[HALO:HALO + owned]
        mixed[...] = (outer[pl.ds(start, owned), :].astype(F32) * convolved).astype(BF16)

        def step(i, carry):
            at = pl.ds(pl.multiple_of(i * tile, tile), tile)
            mpart[pl.ds(start, owned), at] = jnp.dot(
                mixed[...], outw[:, at], preferred_element_type=F32
            ).astype(BF16)
            return carry

        lax.fori_loop(0, features // tile, step, 0)

    for x in range(high):
        mix_rows(x, 1 - low)
        m_core[x].start()

    weigh(weights, at_first, at_second, rw_ref[...])
    own_in.wait()

    def arrive(*ks):
        for k in ks:
            out[k].wait_recv()
        x_out[ks].start()

    arrive(1)
    for x in range(high):
        mix_rows(x, low)
    for x in range(high):
        m_core[x].wait_recv()

    theirs = pl.multiple_of((2 * (1 - top) + low) * owned, 16)

    def sum_across(i, carry):
        at = pl.ds(pl.multiple_of(i * 16, 16), 16)
        mcore[1 - top, at] = (
            mcore[1 - top, at].astype(F32)
            + mpart[pl.ds(pl.multiple_of(theirs + i * 16, 16), 16), :].astype(F32)
        ).astype(BF16)
        return carry

    lax.fori_loop(0, owned // 16, sum_across, 0)
    m_across[0].start()

    def spread(j):
        for ks in groups:
            if stage[ks[0]] == j:
                x_out[ks].wait_recv()
        d_out[j].start()

    def activate(j, hooks):
        d_out[j].wait_recv()

        def step(i, carry):
            for at_step, hook in hooks:
                @pl.when(i == at_step)
                def _():
                    hook()

            at = pl.ds(pl.multiple_of(i * tile, tile), tile)
            x = slots[pl.ds(base[j], 2 * half[j]), :]
            g = jnp.dot(x, gate_w[:, at], preferred_element_type=F32)
            u = jnp.dot(x, up_w[:, at], preferred_element_type=F32)
            hidden[pl.ds(0, 2 * half[j]), at] = (g / (1.0 + jnp.exp(-g)) * u).astype(BF16)
            return carry

        lax.fori_loop(0, gate_w.shape[1] // tile, step, 0)

    def project(j):
        def step(i, carry):
            at = pl.ds(pl.multiple_of(i * tile, tile), tile)
            part[pl.ds(base[j], 2 * half[j]), at] = jnp.dot(
                hidden[pl.ds(0, 2 * half[j]), :], down_w[:, at], preferred_element_type=F32
            ).astype(BF16)
            return carry

        lax.fori_loop(0, down_w.shape[1] // tile, step, 0)
        d_back[j].start()

    def pair_sum(k, of, ref, start):
        j = stage[k]

        def step(i, carry):
            first = of * wide[j] + seat[k] + i * 16
            ref[rows_at(start + i * 16, 16), :] = (
                part[rows_at(own_rows(j) + first, 16), :].astype(F32)
                + core_in[rows_at(part_base[j] + first, 16), :].astype(F32)
            ).astype(BF16)
            return carry

        lax.fori_loop(0, cap // 16, step, 0)

    def pair_up(j):
        d_back[j].wait_recv()
        for k in steps[j]:
            at = part_base[j] + seat[k]
            if k == 0:
                pair_sum(k, top, back, me * cap)
                pair_sum(k, 1 - top, back_in, (me - first_near) * cap)
                continue
            pair_sum(k, 1 - top, core_in, at + (1 - top) * wide[j])
            if k >= near:
                x_back[k].start()
                continue
            home_in[k].start()
            pair_sum(k, top, core_in, at + top * wide[j])
            home[k].start()

    def finish(k):
        j = stage[k]
        x_back[k].wait_recv()

        def step(i, carry):
            here = rows_at((k - near) * cap + i * 16, 16)
            first = top * wide[j] + seat[k] + i * 16
            chip_in[here, :] = (
                part[rows_at(own_rows(j) + first, 16), :].astype(F32)
                + core_in[rows_at(part_base[j] + first, 16), :].astype(F32)
                + chip_in[here, :].astype(F32)
            ).astype(BF16)
            return carry

        lax.fori_loop(0, cap // 16, step, 0)
        home[k].start()

    def finish_all(j):
        for k in steps[j]:
            if k >= near:
                finish(k)

    waiting = sequence(experts)

    def arrive_to(j):
        while any(k in waiting for ks in steps[:j + 1] for k in ks):
            arrive(waiting.pop(0))

    for k in range(2):
        arrive(waiting.pop(0))
    spread(0)
    for copy in routing:
        copy.wait_recv()
    weigh(
        weights_in, *slots_of(routes_in[...], first_near * cap, near * cap), rw_in[...]
    )
    for i in range(stages):
        hooks = []
        if i == 0:
            hooks.append((2, functools.partial(spread, 1)))
            loads[9].wait()
            loads[10].wait()
        else:
            hooks.append((1, functools.partial(arrive_to, i + 2)))
            hooks.append((2, functools.partial(pair_up, i - 1)))
        activate(i, hooks)
        if i == 0:
            arrive_to(2)
            loads[11].wait()
        elif i + 1 < stages:
            spread(i + 1)
        if i == 3:
            finish_all(1)
        project(i)
        if i > 3:
            finish_all(i - 2)
    pair_up(stages - 1)
    for copy in m_across[1:]:
        copy.start()
    finish_all(stages - 2)
    finish_all(stages - 1)
    for k in range(1, near):
        home_in[k].wait_recv()

    def combine_in(i, carry):
        at = pl.ds(pl.multiple_of(i * tile, tile), tile)
        both = jnp.dot(weights_in[...], back_in[:, at], preferred_element_type=F32)
        cross_out[:, at] = (both[:rows_own] + both[rows_own:]).astype(BF16)
        return carry

    lax.fori_loop(0, features // tile, combine_in, 0)
    cross.start()

    for copy in m_across:
        copy.wait_recv()
    mine_rows = pl.multiple_of(mine * owned, 16)

    def sum_own(i, carry):
        at = pl.ds(pl.multiple_of(i * 16, 16), 16)
        mixer_ref[at, :] = (
            mpart[pl.ds(pl.multiple_of(mine_rows + i * 16, 16), 16), :].astype(F32)
            + mcore[top, at].astype(F32)
            + mx_in[at, :].astype(F32)
        ).astype(BF16)
        return carry

    lax.fori_loop(0, owned // 16, sum_own, 0)
    for k in range(1, experts):
        home[k].wait()
    cross.wait()

    def combine(i, carry):
        at = pl.ds(pl.multiple_of(i * tile, tile), tile)
        both = jnp.dot(weights[...], back[:, at], preferred_element_type=F32)
        moe_ref[:, at] = (
            both[:rows_own] + both[rows_own:] + cross_in[:, at].astype(F32)
        ).astype(BF16)
        return carry

    lax.fori_loop(0, features // tile, combine, 0)
    for k in range(1, experts):
        out[k].wait_send()
    for copy in list(x_out.values()) + list(x_back.values()) + list(home_in.values()) + routing:
        copy.wait_send()
    for j in range(stages):
        d_out[j].wait_send()
        d_back[j].wait_send()
    for copy in m_core + m_across:
        copy.wait_send()


def body(
    value_in, gate_in, outer_gate, conv_weight, out_weight, moe_tokens, norm_gain, routes,
    route_weight, expert_gate, expert_up, expert_down,
):
    row_total, top_count = routes.shape
    features = moe_tokens.shape[1]
    length, channels = value_in.shape
    local_units = expert_gate.shape[2]
    experts, shards = lax.axis_size("ep"), lax.axis_size("tp")
    capacity = 3 * top_count * row_total // (2 * experts)
    capacity = -(-capacity // 16) * 16
    slots = experts * capacity
    steps = paired(experts)
    stages, total = len(steps), slots * shards
    owned = length // shards
    dma = pltpu.SemaphoreType.DMA
    vmem, hbm = pl.BlockSpec(memory_space=pltpu.VMEM), pl.BlockSpec(memory_space=pl.ANY)
    return pl.pallas_call(
        functools.partial(kernel, experts, shards, capacity, 512),
        out_shape=(
            jax.ShapeDtypeStruct((owned, features), BF16),
            jax.ShapeDtypeStruct((row_total, features), BF16),
        ),
        in_specs=[hbm] * 12,
        out_specs=(vmem, vmem),
        scratch_shapes=[
            pltpu.VMEM((features, local_units), BF16),
            pltpu.VMEM((features, local_units), BF16),
            pltpu.VMEM((local_units, features), BF16),
            pltpu.VMEM((length, channels), BF16),
            pltpu.VMEM((length, channels), BF16),
            pltpu.VMEM((length, channels), BF16),
            pltpu.VMEM((channels, features), BF16),
            pltpu.VMEM((row_total, features), BF16),
            pltpu.VMEM(conv_weight.shape, BF16),
            pltpu.VMEM(norm_gain.shape, BF16),
            pltpu.VMEM((top_count, row_total), jnp.int32),
            pltpu.VMEM((top_count, row_total), F32),
            pltpu.VMEM((top_count, row_total), jnp.int32),
            pltpu.VMEM((top_count, row_total), F32),
            pltpu.VMEM((row_total, features), BF16),
            pltpu.VMEM((slots, features), BF16),
            pltpu.VMEM((2 * row_total, slots), BF16),
            pltpu.VMEM((2 * row_total, slots // 2), BF16),
            pltpu.VMEM((total, features), BF16),
            pltpu.VMEM((2 * shards * capacity, local_units), BF16),
            pltpu.VMEM((total, features), BF16),
            pltpu.VMEM((total // 2, features), BF16),
            pltpu.VMEM((slots // 2, features), BF16),
            pltpu.VMEM((slots, features), BF16),
            pltpu.VMEM((slots // 2, features), BF16),
            pltpu.VMEM((row_total, features), BF16),
            pltpu.VMEM((row_total, features), BF16),
            pltpu.VMEM((length + 2 * HALO, channels), BF16),
            pltpu.VMEM((owned, channels), BF16),
            pltpu.VMEM((length, features), BF16),
            pltpu.VMEM((shards // 2, owned, features), BF16),
            pltpu.VMEM((owned, features), BF16),
            dma((12,)),
            dma((1,)),
        ]
        + [dma((experts,))] * 4
        + [dma((stages,))] * 4
        + [dma((experts,))] * 4
        + [dma((2,))] * 4
        + [dma((len(PIECES),))] * 2
        + [dma((2,))] * 2
        + [dma((experts // 2,))] * 2
        + [dma((1,))] * 2,
        compiler_params=pltpu.CompilerParams(
            collective_id=0, has_side_effects=True, vmem_limit_bytes=67043328
        ),
        cost_estimate=pl.CostEstimate(
            flops=6 * total * features * local_units,
            bytes_accessed=6 * features * local_units,
            transcendentals=total * local_units,
        ),
    )(
        value_in, gate_in, outer_gate, conv_weight, out_weight, moe_tokens,
        norm_gain, routes.T, route_weight.T,
        expert_gate[0], expert_up[0], expert_down[0],
    )


def solution(mesh):
    placed = (
        P("ep", "tp"),
        P("ep", "tp"),
        P("ep", "tp"),
        P(None, "tp"),
        P("tp", None),
        P(("ep", "tp"), None),
        P(),
        P(("ep", "tp"), None),
        P(("ep", "tp"), None),
        P("ep", None, "tp"),
        P("ep", None, "tp"),
        P("ep", "tp", None),
    )
    return jax.shard_map(
        body,
        mesh=mesh,
        in_specs=placed,
        out_specs=(P(("ep", "tp"), None), P(("ep", "tp"), None)),
        check_vma=False,
    )
```

time: 106 us -> 98 us (0.925)
  Pallas kernels: 97.5 us -> 93.3 us
  local copies, waits for them, and re-layouts: 7.88 us -> 3.76 us
    pallas_call x1, Pallas kernels: 97.5 us -> 93.3 us  [body(): pl.pallas_call(functools.partial(kernel, experts, shards, capacity, 512),...]
    unnamed x4 -> x2, local copies, waits for them, and re-layouts: 6.59 us -> 3.76 us
    reshape x1 -> x0, local copies, waits for them, and re-layouts: 1.29 us -> none  [body(): norm_gain.reshape(1, features)]
where the time goes in v2:
time: 98 us; the launch traced here: 97.7 us
  Pallas kernels  93.3 us (95%)
  local copies, waits for them, and re-layouts  3.76 us (4%)
    pallas_call x1, Pallas kernels, body(): pl.pallas_call(functools.partial(kernel, experts, shards, capacity, 512),...  93.3 us
    unnamed x2, local copies, waits for them, and re-layouts  3.76 us

profile of v2, /device:TPU:0, one launch (start us, length us, event | category | flops | bytes accessed | tf_op | source)
XLA Modules:
  0.0 97.7 jit_solution(2136336364403933017)
XLA Ops:
  0.6 93.3 %shard_map.131 = (bf16[128,2048]{1,0:T(8,128)(2,1)}, bf16[128,2048]{1,0:T(8,128)(2,1)}) custom-call(bf16[512,256]{1,0:T(8,128)(2,1)} %value_hbm.1, bf16[512,256]{1,0:T(8,128)(2,1)} %gatein_hbm.1, bf16[512,256]{1,0:T(8,128)(2,1)} %outer_hbm.1, bf16[3,256]{1,0:T(4,128)(2,1)} %conv_hbm.1, bf16[256,2048]{1,0:T(8,128)(2,1)} %outw_hbm.1, ...), custom_call_target="tpu_custom_call" | custom-call | flops 28991029248 | bytes 18874368 | tf_op jit(solution)/shard_map/pallas_call | solution.py:528
  94.0 1.9 %copy.16 = bf16[128,2048]{1,0:T(8,128)(2,1)} copy(bf16[128,2048]{1,0:T(8,128)(2,1)} %get-tuple-element.4) | data formatting | bytes 1048576
  95.9 1.9 %copy.17 = bf16[128,2048]{1,0:T(8,128)(2,1)} copy(bf16[128,2048]{1,0:T(8,128)(2,1)} %get-tuple-element.5) | data formatting | bytes 1048576

commit v3 on v2

--- a/solution.py
+++ b/solution.py
@@ -42,7 +42,7 @@
     experts, shards, cap, tile,
     value_hbm, gatein_hbm, outer_hbm, conv_hbm, outw_hbm, tokens_hbm, gain_hbm, routes_hbm, rw_hbm,
     gate_hbm, up_hbm, down_hbm,
-    mixer_ref, moe_ref,
+    both_ref,
     gate_w, up_w, down_w, value, gatein, outer, outw, tokens, conv_ref, gain_ref, routes_ref, rw_ref,
     routes_in, rw_in, normed, sent, weights, weights_in, slots, hidden, part, core_in, chip_in,
     back, back_in, cross_out, cross_in,
@@ -359,13 +359,13 @@
 
     def project(j):
         def step(i, carry):
-            at = pl.ds(pl.multiple_of(i * tile, tile), tile)
+            at = pl.ds(pl.multiple_of(i * 2 * tile, 2 * tile), 2 * tile)
             part[pl.ds(base[j], 2 * half[j]), at] = jnp.dot(
                 hidden[pl.ds(0, 2 * half[j]), :], down_w[:, at], preferred_element_type=F32
             ).astype(BF16)
             return carry
 
-        lax.fori_loop(0, down_w.shape[1] // tile, step, 0)
+        lax.fori_loop(0, down_w.shape[1] // (2 * tile), step, 0)
         d_back[j].start()
 
     def pair_sum(k, of, ref, start):
@@ -476,7 +476,7 @@
 
     def sum_own(i, carry):
         at = pl.ds(pl.multiple_of(i * 16, 16), 16)
-        mixer_ref[at, :] = (
+        both_ref[at, :] = (
             mpart[pl.ds(pl.multiple_of(mine_rows + i * 16, 16), 16), :].astype(F32)
             + mcore[top, at].astype(F32)
             + mx_in[at, :].astype(F32)
@@ -491,7 +491,7 @@
     def combine(i, carry):
         at = pl.ds(pl.multiple_of(i * tile, tile), tile)
         both = jnp.dot(weights[...], back[:, at], preferred_element_type=F32)
-        moe_ref[:, at] = (
+        both_ref[pl.ds(owned, rows_own), at] = (
             both[:rows_own] + both[rows_own:] + cross_in[:, at].astype(F32)
         ).astype(BF16)
         return carry
@@ -525,14 +525,11 @@
     owned = length // shards
     dma = pltpu.SemaphoreType.DMA
     vmem, hbm = pl.BlockSpec(memory_space=pltpu.VMEM), pl.BlockSpec(memory_space=pl.ANY)
-    return pl.pallas_call(
+    both = pl.pallas_call(
         functools.partial(kernel, experts, shards, capacity, 512),
-        out_shape=(
-            jax.ShapeDtypeStruct((owned, features), BF16),
-            jax.ShapeDtypeStruct((row_total, features), BF16),
-        ),
+        out_shape=jax.ShapeDtypeStruct((owned + row_total, features), BF16),
         in_specs=[hbm] * 12,
-        out_specs=(vmem, vmem),
+        out_specs=vmem,
         scratch_shapes=[
             pltpu.VMEM((features, local_units), BF16),
             pltpu.VMEM((features, local_units), BF16),
@@ -590,6 +587,7 @@
         norm_gain, routes.T, route_weight.T,
         expert_gate[0], expert_up[0], expert_down[0],
     )
+    return both[:owned], both[owned:]
 
 
 def solution(mesh):

time: 98 us -> 96.4 us (0.984)
  local copies, waits for them, and re-layouts: 3.76 us -> 2.28 us
    unnamed x2 -> x0, local copies, waits for them, and re-layouts: 3.76 us -> none
    slice x0 -> x1, local copies, waits for them, and re-layouts: none -> 2.28 us  [body(): return (both[:owned], both[owned:])]
where the time goes in v3:
time: 96.4 us; the launch traced here: 96.3 us
  Pallas kernels  93.3 us (97%)
  local copies, waits for them, and re-layouts  2.28 us (2%)
    pallas_call x1, Pallas kernels, body(): pl.pallas_call(functools.partial(kernel, experts, shards, capacity, 512),...  93.3 us
    slice x1, local copies, waits for them, and re-layouts, body(): return (both[:owned], both[owned:])  2.28 us

profile of v3, /device:TPU:0, one launch (start us, length us, event | category | flops | bytes accessed | tf_op | source)
XLA Modules:
  0.0 96.3 jit_solution(10153732665098450191)
XLA Ops:
  0.6 93.3 %shard_map.131 = bf16[256,2048]{1,0:T(8,128)(2,1)} custom-call(bf16[512,256]{1,0:T(8,128)(2,1)} %value_hbm.1, bf16[512,256]{1,0:T(8,128)(2,1)} %gatein_hbm.1, bf16[512,256]{1,0:T(8,128)(2,1)} %outer_hbm.1, bf16[3,256]{1,0:T(4,128)(2,1)} %conv_hbm.1, bf16[256,2048]{1,0:T(8,128)(2,1)} %outw_hbm.1, bf16[128,2048]{1,0:T(8,128)(2,1)} %tokens_hbm.1, ...), custom_call_target="tpu_custom_call" | custom-call | flops 28991029248 | bytes 18874368 | tf_op jit(solution)/shard_map/pallas_call | solution.py:528
  94.0 2.3 %fusion = (bf16[128,2048]{1,0:T(8,128)(2,1)}, bf16[128,2048]{1,0:T(8,128)(2,1)}) fusion(bf16[256,2048]{1,0:T(8,128)(2,1)} %shard_map.131), kind=kLoop, calls=%fused_computation | loop fusion | bytes 2097152 | tf_op jit(solution)/shard_map/slice | solution.py:590
